TPU v7x, 32 devices: a whole 2x2x4 slice. The times are simulated.
32 devices in a mesh: ra: 8 (over z, y), cb: 4 (over x, core).
Axes of the slice: x: 2, y: 2, z: 4, core: 2. Of those that a mesh axis runs over, the one named last changes fastest.
Arguments:
- tokens: bfloat16 [4, 128, 4096], P(None, None, 'ra'), may hold values from -64 to 64
- norm_gain: float32 [2, 4096], P(None, 'ra'), may hold values from 0.1 to 1.9
- gate_weight: bfloat16 [2, 4096, 11264], P(None, 'ra', 'cb'), may hold values from -0.09375 to 0.09375
- up_weight: bfloat16 [2, 4096, 11264], P(None, 'ra', 'cb'), may hold values from -0.09375 to 0.09375
- gate_taps: float32 [2, 3, 11264], P(None, None, 'cb'), may hold values from -3 to 3
- up_taps: float32 [2, 3, 11264], P(None, None, 'cb'), may hold values from -3 to 3
- gate_bias: float32 [2, 11264], P(None, 'cb'), may hold values from -3 to 3
- up_bias: float32 [2, 11264], P(None, 'cb'), may hold values from -3 to 3
- down_weight: bfloat16 [2, 11264, 4096], P(None, 'cb', 'ra'), may hold values from -0.0546875 to 0.0546875
Outputs:
- mixed: bfloat16 [4, 128, 4096], P(None, None, 'ra')
All inputs are finite; a program needn't handle non-finite values.
Results may differ from a plain program's by a relative error of at most 0.03.
Values may be sent and summed in bfloat16 or wider, within the bound.
A program may use at most 64 MiB of HBM per device.

v0:
```python
import jax
import jax.numpy as jnp
from jax import lax
from jax.sharding import PartitionSpec as P

D = 4096
KERNEL = 3
LAYERS = 2


eps = 1e-06
resid_scale = 0.5


def causal_conv(projected, kernel, offsets, seqs, length):
    values = projected.astype(jnp.float32).reshape(seqs, length, 2, projected.shape[2])
    padded = jnp.pad(values, ((0, 0), (KERNEL - 1, 0), (0, 0), (0, 0)))
    result = offsets
    for tap_idx in range(KERNEL):
        result = result + kernel[tap_idx] * padded[:, tap_idx : tap_idx + length]
    return result.reshape(seqs * length, 2, projected.shape[2])


def per_device(
    tokens, norm_gain, gate_weight, up_weight, gate_taps, up_taps, gate_bias, up_bias, down_weight
):
    seqs, length, width_local = tokens.shape
    rows_count = seqs * length
    carried = tokens.reshape(rows_count, width_local).astype(jnp.float32)
    for layer_idx in range(LAYERS):
        local_squares = jnp.sum(carried * carried, axis=1)
        scaled = (carried * norm_gain[layer_idx]).astype(jnp.bfloat16)
        kernel = jnp.stack([gate_taps[layer_idx], up_taps[layer_idx]], axis=1)
        offsets = jnp.stack([gate_bias[layer_idx], up_bias[layer_idx]], axis=0)
        down_local = down_weight[layer_idx]
        partial_value = jnp.stack(
            [
                jnp.dot(scaled, gate_weight[layer_idx], preferred_element_type=jnp.float32),
                jnp.dot(scaled, up_weight[layer_idx], preferred_element_type=jnp.float32),
            ],
            axis=1,
        )
        row_squares = lax.psum(local_squares, "ra")
        summed = lax.psum(partial_value.astype(jnp.bfloat16), "ra").astype(jnp.float32)
        inverse = lax.rsqrt(row_squares / D + eps)
        projected = (summed * inverse[:, None, None]).astype(jnp.bfloat16)
        convolved = causal_conv(projected, kernel, offsets, seqs, length)
        hidden = (jax.nn.silu(convolved[:, 0]) * convolved[:, 1]).astype(jnp.bfloat16)
        branch_part = jnp.dot(hidden, down_local, preferred_element_type=jnp.float32)
        branch = lax.psum(branch_part.astype(jnp.bfloat16), "cb").astype(jnp.float32)
        carried = resid_scale * carried + branch
    return carried.astype(jnp.bfloat16).reshape(seqs, length, width_local)


def solution(mesh):
    in_specs = (
        P(None, None, "ra"),
        P(None, "ra"),
        P(None, "ra", "cb"),
        P(None, "ra", "cb"),
        P(None, None, "cb"),
        P(None, None, "cb"),
        P(None, "cb"),
        P(None, "cb"),
        P(None, "cb", "ra"),
    )
    out_specs = P(None, None, "ra")
    return jax.shard_map(
        per_device, mesh=mesh, in_specs=in_specs, out_specs=out_specs, check_vma=False
    )
```

profile of v0, /device:TPU:1, one launch (start us, length us, event | category | flops | bytes accessed | tf_op | source)
XLA Modules:
  0.0 537.5 jit_solution(4109739938134989243)
XLA Ops:
  6.5 0.0 all-reduce.7.cloned.1.call-start
  6.5 0.0 copy-start.5
  6.5 0.9 fusion.60
  7.4 1.5 convert_multiply_fusion.2
  8.9 3.5 fusion.13
  12.3 0.0 copy-done.5
  12.4 1.7 fusion.12
  14.0 3.0 pad_maximum_fusion
  17.1 0.0 copy-start.3
  17.1 0.0 copy-start.4
  17.1 0.0 copy-start.1
  17.1 0.0 copy-start.2
  17.1 0.0 all-reduce.7.cloned.1.call-update
  17.1 0.0 all-reduce.9.cloned.1.call-start
  17.1 19.5 %psum.43 = f32[512]{0:T(512)S(1)} all-reduce(f32[512]{0:T(512)S(1)} %bitcast.89), channel_id=1, replica_groups=mesh['ra'=8,'cb'=4] {'ra'}, use_global_device_ids=true, to_apply=%region_2.0 | all-reduce | flops 512 | bytes 4096 | tf_op jit(solution)/shard_map/psum | solution.py:43
  36.7 0.0 copy-done.3
  36.7 0.0 copy-done.4
  36.8 0.0 copy-done.1
  36.8 0.0 copy-done.2
  36.8 0.1 slice_bitcast_fusion
  36.9 0.1 fusion.52
  37.0 180.7 %all-reduce.7.cloned.1.call-done = bf16[512,2,2816]{2,0,1:T(8,128)(2,1)} async-done(((bf16[512,2,2816]{2,0,1:T(8,128)(2,1)}), bf16[512,2,2816]{2,0,1:T(8,128)(2,1)}) %all-reduce.7.cloned.1.call-update) | async-done | bytes 5767184 | tf_op jit(solution)/shard_map/psum | solution.py:44
  217.7 4.2 multiply_convert_fusion.1
  221.9 0.0 slice-start
  221.9 1.0 convert.22
  223.0 0.0 slice-start.1
  223.0 6.3 %fusion.3 = f32[4,128,2,2816]{3,1,0,2:T(8,128)} fusion(f32[4,128,2,2816]{3,1,0,2:T(8,128)S(1)} %convert.22, f32[2,2816]{1,0:T(2,128)S(1)} %get-tuple-element.18, f32[2,2816]{1,0:T(2,128)S(1)} %get-tuple-element.19, f32[2,2816]{1,0:T(2,128)S(1)} %get-tuple-element.17, f32[2,2816]{1,0:T(2,128)S(1)} %get-tuple-element.28), kind=kLoop, calls=%fused_computation.7 | loop fusion | flops 17301504 | bytes 23158784 | tf_op jit(solution)/shard_map/add | solution.py:20
  229.3 0.0 slice-done
  229.3 0.0 slice-done.1
  229.3 6.9 %fusion.34 = bf16[512,512]{1,0:T(8,128)(2,1)} fusion(bf16[2,2816,512]{2,1,0:T(8,128)(2,1)S(1)} %bitcast.93, f32[512,2,2816]{2,0,1:T(8,128)} %bitcast.85), kind=kOutput, calls=%fused_computation.49 | convolution fusion | flops 1485307904 | bytes 14942208 | tf_op jit(solution)/shard_map/dot_general | solution.py:49
  236.2 0.0 all-reduce.9.cloned.1.call-update
  236.2 0.2 all-reduce.11.cloned.1.call-start
  236.4 31.3 %all-reduce.9.cloned.1.call-done = bf16[512,512]{1,0:T(8,128)(2,1)} async-done(((bf16[512,512]{1,0:T(8,128)(2,1)}), bf16[512,512]{1,0:T(8,128)(2,1)}) %all-reduce.9.cloned.1.call-update) | async-done | bytes 524304 | tf_op jit(solution)/shard_map/psum | solution.py:50
  267.7 1.3 multiply_reduce_fusion
  269.0 3.5 fusion.15
  272.5 3.5 fusion.14
  276.0 3.0 pad_maximum_fusion.1
  279.0 0.0 all-reduce.11.cloned.1.call-update
  279.1 0.0 all-reduce.13.cloned.1.call-start
  279.1 0.1 fusion.54
  279.2 18.6 %psum.46 = f32[512]{0:T(512)S(1)} all-reduce(f32[512]{0:T(512)S(1)} %get-tuple-element.5), channel_id=1, replica_groups=mesh['ra'=8,'cb'=4] {'ra'}, use_global_device_ids=true, to_apply=%region_6.7 | all-reduce | flops 512 | bytes 4096 | tf_op jit(solution)/shard_map/psum | solution.py:43
  297.8 181.0 %all-reduce.11.cloned.1.call-done = bf16[512,2,2816]{2,0,1:T(8,128)(2,1)} async-done(((bf16[512,2,2816]{2,0,1:T(8,128)(2,1)}), bf16[512,2,2816]{2,0,1:T(8,128)(2,1)}) %all-reduce.11.cloned.1.call-update) | async-done | bytes 5767184 | tf_op jit(solution)/shard_map/psum | solution.py:44
  478.9 4.2 multiply_convert_fusion
  483.1 0.0 slice-start.2
  483.1 1.0 convert.23
  484.1 0.0 slice-start.3
  484.1 6.3 %fusion.8 = f32[4,128,2,2816]{3,1,0,2:T(8,128)} fusion(f32[4,128,2,2816]{3,1,0,2:T(8,128)S(1)} %convert.23, f32[2,2816]{1,0:T(2,128)S(1)} %get-tuple-element.11, f32[2,2816]{1,0:T(2,128)S(1)} %get-tuple-element.12, f32[2,2816]{1,0:T(2,128)S(1)} %get-tuple-element.10, f32[2,2816]{1,0:T(2,128)S(1)} %get-tuple-element.29), kind=kLoop, calls=%fused_computation.12 | loop fusion | flops 17301504 | bytes 23158784 | tf_op jit(solution)/shard_map/add | solution.py:20
  490.4 0.0 slice-done.2
  490.4 0.0 slice-done.3
  490.4 0.0 copy-start
  490.4 7.0 %fusion.39 = bf16[512,512]{1,0:T(8,128)(2,1)} fusion(bf16[2,2816,512]{2,1,0:T(8,128)(2,1)S(1)} %bitcast.95, f32[512,2,2816]{2,0,1:T(8,128)} %bitcast.86), kind=kOutput, calls=%fused_computation.50 | convolution fusion | flops 1485307904 | bytes 14942208 | tf_op jit(solution)/shard_map/dot_general | solution.py:49
  497.4 0.0 all-reduce.13.cloned.1.call-update
  497.4 31.5 %all-reduce.13.cloned.1.call-done = bf16[512,512]{1,0:T(8,128)(2,1)} async-done(((bf16[512,512]{1,0:T(8,128)(2,1)}), bf16[512,512]{1,0:T(8,128)(2,1)}) %all-reduce.13.cloned.1.call-update) | async-done | bytes 524304 | tf_op jit(solution)/shard_map/psum | solution.py:50
  528.9 0.0 copy-done
  528.9 2.0 add_convert_fusion
  (7 shorter events, 0.1 us)
Async XLA Ops:
  6.5 211.2 %all-reduce.7.cloned.1.call-start = ((), (), s32[]{:S(2)}) async-start(), calls=%async_computation | async-start | bytes 11534336 | tf_op jit(solution)/shard_map/psum | solution.py:44
  6.5 5.8 %copy-start.5 = (bf16[2,512,2816]{2,1,0:T(8,128)(2,1)S(1)}, bf16[2,512,2816]{2,1,0:T(8,128)(2,1)}, u32[]{:S(2)}) copy-start(bf16[2,512,2816]{2,1,0:T(8,128)(2,1)} %param.11) | copy-start | bytes 17301508
  17.1 19.6 %copy-start.3 = (f32[2,2816]{1,0:T(2,128)S(1)}, f32[2,2816]{1,0:T(2,128)}, u32[]{:S(2)}) copy-start(f32[2,2816]{1,0:T(2,128)} %param.15) | copy-start | bytes 67588
  17.1 19.7 %copy-start.4 = (f32[2,2816]{1,0:T(2,128)S(1)}, f32[2,2816]{1,0:T(2,128)}, u32[]{:S(2)}) copy-start(f32[2,2816]{1,0:T(2,128)} %param.16) | copy-start | bytes 67588
  17.1 19.7 %copy-start.1 = (f32[2,3,2816]{2,0,1:T(2,128)S(1)}, f32[2,3,2816]{2,0,1:T(2,128)}, u32[]{:S(2)}) copy-start(f32[2,3,2816]{2,0,1:T(2,128)} %param.14) | copy-start | bytes 202756
  17.1 19.8 %copy-start.2 = (f32[2,3,2816]{2,0,1:T(2,128)S(1)}, f32[2,3,2816]{2,0,1:T(2,128)}, u32[]{:S(2)}) copy-start(f32[2,3,2816]{2,0,1:T(2,128)} %param.13) | copy-start | bytes 202756
  17.1 250.6 %all-reduce.9.cloned.1.call-start = ((), (), s32[]{:S(2)}) async-start(), calls=%async_computation.1 | async-start | bytes 1048576 | tf_op jit(solution)/shard_map/psum | solution.py:50
  221.9 7.3 %slice-start = ((s8[5767168]{0:T(1024)(128)(4,1)}), s8[1572864]{0:T(1024)(128)(4,1)S(1)}, s32[]{:S(2)}) async-start(s8[5767168]{0:T(1024)(128)(4,1)} %bitcast.92), calls=%async_computation.4 | async-start | bytes 3145728
  223.0 6.3 %slice-start.1 = ((s8[5767168]{0:T(1024)(128)(4,1)}), s8[4194304]{0:T(1024)(128)(4,1)S(1)}, s32[]{:S(2)}) async-start(s8[5767168]{0:T(1024)(128)(4,1)} %bitcast.92), calls=%async_computation.5 | async-start | bytes 8388608
  236.2 242.6 %all-reduce.11.cloned.1.call-start = ((), (), s32[]{:S(2)}) async-start(), calls=%async_computation.2 | async-start | bytes 11534336 | tf_op jit(solution)/shard_map/psum | solution.py:44
  279.1 249.9 %all-reduce.13.cloned.1.call-start = ((), (), s32[]{:S(2)}) async-start(), calls=%async_computation.3 | async-start | bytes 1048576 | tf_op jit(solution)/shard_map/psum | solution.py:50
  483.1 7.3 %slice-start.2 = ((s8[5767168]{0:T(1024)(128)(4,1)}), s8[1572864]{0:T(1024)(128)(4,1)S(1)}, s32[]{:S(2)}) async-start(s8[5767168]{0:T(1024)(128)(4,1)} %bitcast.94), calls=%async_computation.6 | async-start | bytes 3145728
  484.1 6.3 %slice-start.3 = ((s8[5767168]{0:T(1024)(128)(4,1)}), s8[4194304]{0:T(1024)(128)(4,1)S(1)}, s32[]{:S(2)}) async-start(s8[5767168]{0:T(1024)(128)(4,1)} %bitcast.94), calls=%async_computation.7 | async-start | bytes 8388608
  490.4 38.5 %copy-start = (bf16[512,512]{1,0:T(8,128)(2,1)S(1)}, bf16[512,512]{1,0:T(8,128)(2,1)}, u32[]{:S(2)}) copy-start(bf16[512,512]{1,0:T(8,128)(2,1)} %all-reduce.9.cloned.1.call-done) | copy-start | bytes 1572868
Sparse Core Ops, SparseCore 0:
  17.2 200.4 all-reduce.6
  236.3 31.3 all-reduce.8
  279.2 199.6 all-reduce.10
  497.5 31.3 all-reduce.12
where the time goes:
time: 540 us; the launch traced here: 538 us
  waiting for transfers between devices  425 us (79%)
  blocking collectives  38.2 us (7%)
  other arithmetic  34.1 us (6%)
  matrix products  26 us (5%)
  between operations  13.3 us (2%)
    psum x2, waiting for transfers between devices, per_device(): lax.psum(partial_value.astype(jnp.bfloat16), 'ra').astype(jnp.float32)  362 us
    psum x2, waiting for transfers between devices, per_device(): lax.psum(branch_part.astype(jnp.bfloat16), 'cb').astype(jnp.float32)  62.8 us
    psum x2, blocking collectives, per_device(): row_squares = lax.psum(local_squares, 'ra')  38.2 us
    dot_general x2, matrix products, per_device(): jnp.dot(hidden, down_local, preferred_element_type=jnp.float32)  13.9 us
    add x2, other arithmetic, causal_conv(): result = result + kernel[tap_idx] * padded[:, tap_idx:tap_idx + length]  12.5 us
  transfers between devices with their start and end apart: 4, of which 4 were waited for; matrix products, arithmetic and copies ran while one was open for 0% of the time, Pallas kernels for 0%

commit v1 on v0

v1 whole, which is shorter than its diff:
```python
import functools

import jax
import jax.numpy as jnp
from jax import lax
from jax.experimental import pallas as pl
from jax.experimental.pallas import tpu as pltpu
from jax.sharding import PartitionSpec as P

EPS = 1e-06
RESID = 0.5
LAG_B, LAG_C, LAG_D, LAG_E = 1, 3, 5, 6

MESH = pl.DeviceIdType.MESH
F32, BF16 = jnp.float32, jnp.bfloat16


def kernel(
    dims,
    tok_ref, gain_ref, gw_hbm, uw_hbm, gt_ref, ut_ref, gb_ref, ub_ref, dw_hbm,
    out_ref,
    gw_ref, uw_ref, dw_ref, carried, scaled, inv, tmp, acc,
    sq_own, sq_in, part, y_in, zpart, z_in, hid, c_out, c_in, c_all,
    w_sem, sq_s, sq_r, y_s, y_r, z_s, z_r, hz_s, hz_r, hy_s, hy_r, c_s, c_r, ca_s, ca_r,
):
    n_ra, n_cb, nz, seqs, length, layers, width, chunks = dims
    ny = n_ra // nz
    rows = seqs * length
    part_rows = length // ny
    cb_rows = rows // n_cb
    me_ra = lax.axis_index("ra")
    me_cb = lax.axis_index("cb")
    me_z, me_y = me_ra // ny, me_ra % ny

    def weight_copies(layer):
        return [
            pltpu.make_async_copy(src.at[layer], dst.at[layer], w_sem.at[layer, k])
            for k, (src, dst) in enumerate(
                [(gw_hbm, gw_ref), (uw_hbm, uw_ref), (dw_hbm, dw_ref)]
            )
        ]

    for layer in range(layers):
        for copy in weight_copies(layer):
            copy.start()

    barrier = pltpu.get_barrier_semaphore()
    for step in range(1, n_ra):
        pl.semaphore_signal(
            barrier, inc=1, device_id={"ra": lax.rem(me_ra + step, n_ra)}, device_id_type=MESH
        )
    for step in range(1, n_cb):
        pl.semaphore_signal(
            barrier, inc=1, device_id={"cb": lax.rem(me_cb + step, n_cb)}, device_id_type=MESH
        )
    pl.semaphore_wait(barrier, n_ra + n_cb - 2)

    def remote(src, dst, send, recv, **where):
        return pltpu.make_async_remote_copy(
            src_ref=src, dst_ref=dst, send_sem=send, recv_sem=recv,
            device_id=where, device_id_type=MESH,
        )

    def square_copy(step):
        return remote(
            sq_own, sq_in.at[step - 1], sq_s.at[step - 1], sq_r.at[step - 1],
            ra=lax.rem(me_ra + step, n_ra),
        )

    def y_copy(i, step):
        to = lax.rem(me_y + step, ny)
        return remote(
            part.at[i, to], y_in.at[i, step - 1], y_s.at[i, step - 1], y_r.at[i, step - 1],
            ra=me_z * ny + to,
        )

    def z_copy(i, step):
        to = lax.rem(me_z + step, nz)
        return remote(
            zpart.at[i, to], z_in.at[i, step - 1], z_s.at[i, step - 1], z_r.at[i, step - 1],
            ra=to * ny + me_y,
        )

    def hz_copy(i, step, z):
        to = lax.rem(me_z + step, nz)
        block = hid.at[i, me_y, z]
        return remote(
            block, block, hz_s.at[i, step - 1], hz_r.at[i, step - 1], ra=to * ny + me_y
        )

    def hy_copy(i, step, y):
        to = lax.rem(me_y + step, ny)
        block = hid.at[i, y]
        return remote(
            block, block, hy_s.at[i, step - 1], hy_r.at[i, step - 1], ra=me_z * ny + to
        )

    def c_copy(step):
        to = lax.rem(me_cb + step, n_cb)
        return remote(c_out.at[to], c_in.at[step - 1], c_s.at[step - 1], c_r.at[step - 1], cb=to)

    def ca_copy(step, block):
        to = lax.rem(me_cb + step, n_cb)
        return remote(
            c_all.at[block], c_all.at[block], ca_s.at[step - 1], ca_r.at[step - 1], cb=to
        )

    carried[...] = tok_ref[...].astype(F32)
    row_in_seq = lax.broadcasted_iota(jnp.int32, (length, width), 0)

    def one_layer(layer, _):
        values = carried[...]
        squares = jnp.sum(values * values, axis=1, keepdims=True)
        sq_own[...] = jnp.transpose(jnp.broadcast_to(squares, (rows, 128)))[:8]
        for step in range(1, n_ra):
            square_copy(step).start()
        scaled[...] = (values * gain_ref[layer]).astype(BF16)
        acc[...] = jnp.zeros_like(acc)
        for copy in weight_copies(layer):
            copy.wait()
        total = sq_own[...]
        for step in range(1, n_ra):
            square_copy(step).wait()
            total = total + sq_in[step - 1]
        total = jnp.transpose(jnp.concatenate([total] * 16, axis=0))
        inv[...] = lax.rsqrt(total / (n_ra * gain_ref.shape[2]) + EPS)

        def project(i):
            cols = pl.ds(pl.multiple_of(i * width, width), width)
            for half, (w_ref, taps) in enumerate([(gw_ref, gt_ref), (uw_ref, ut_ref)]):
                lanes = slice(half * width, (half + 1) * width)
                tmp[...] = jnp.dot(
                    scaled[...], w_ref[layer, :, cols], preferred_element_type=F32
                )
                tap = [taps[layer, pl.ds(k, 1), cols] for k in range(3)]
                for s in range(seqs):
                    span = slice(s * length, (s + 1) * length)
                    pre = tmp[span, :] * inv[span, :1]
                    last = jnp.where(row_in_seq >= 1, pltpu.roll(pre, 1, 0), 0.0)
                    older = jnp.where(row_in_seq >= 2, pltpu.roll(pre, 2, 0), 0.0)
                    conv = (tap[0] * older + tap[1] * last + tap[2] * pre).astype(BF16)
                    for y in range(ny):
                        part[i, y, s, :, lanes] = conv[y * part_rows : (y + 1) * part_rows]
            for step in range(1, ny):
                y_copy(i, step).start()

        def add_y(i):
            for step in range(1, ny):
                y_copy(i, step).wait_recv()
            for s in range(seqs):
                value = part[i, me_y, s].astype(F32)
                for step in range(1, ny):
                    value = value + y_in[i, step - 1, s].astype(F32)
                zpart[i, s] = value.astype(BF16)
            for step in range(1, nz):
                z_copy(i, step).start()

        def activate(i):
            cols = pl.ds(pl.multiple_of(i * width, width), width)
            for step in range(1, nz):
                z_copy(i, step).wait_recv()
            value = zpart[i, me_z].astype(F32)
            for step in range(1, nz):
                value = value + z_in[i, step - 1].astype(F32)
            gate = value[:, :width] + gb_ref[layer, :, cols]
            up = value[:, width:] + ub_ref[layer, :, cols]
            hid[i, me_y, me_z] = (gate / (1.0 + jnp.exp(-gate)) * up).astype(BF16)
            for step in range(1, nz):
                hz_copy(i, step, me_z).start()

        def spread_y(i):
            for step in range(1, nz):
                hz_copy(i, step, lax.rem(me_z - step + nz, nz)).wait_recv()
            for step in range(1, ny):
                hy_copy(i, step, me_y).start()

        def down(i):
            depth = pl.ds(pl.multiple_of(i * width, width), width)
            for step in range(1, ny):
                hy_copy(i, step, lax.rem(me_y - step + ny, ny)).wait_recv()
            acc[...] += jnp.dot(
                hid[i].reshape(rows, width), dw_ref[layer, depth, :], preferred_element_type=F32
            )

        def body(t, _):
            for lag, stage in [
                (0, project), (LAG_B, add_y), (LAG_C, activate), (LAG_D, spread_y), (LAG_E, down)
            ]:
                i = t - lag

                @pl.when((i >= 0) & (i < chunks))
                def _():
                    stage(i)

            return 0

        lax.fori_loop(0, chunks + LAG_E, body, 0)

        c_out[...] = acc[...].astype(BF16).reshape(c_out.shape)
        for step in range(1, n_cb):
            c_copy(step).start()

        def settle(i, _):
            for step in range(1, ny):
                y_copy(i, step).wait_send()
                hy_copy(i, step, me_y).wait_send()
            for step in range(1, nz):
                z_copy(i, step).wait_send()
                hz_copy(i, step, me_z).wait_send()
            return 0

        lax.fori_loop(0, chunks, settle, 0)

        value = acc[pl.ds(pl.multiple_of(me_cb * cb_rows, cb_rows), cb_rows), :]
        for step in range(1, n_cb):
            c_copy(step).wait()
            value = value + c_in[step - 1].astype(F32)
        c_all[me_cb] = value.astype(BF16)
        for step in range(1, n_cb):
            ca_copy(step, me_cb).start()
        for step in range(1, n_cb):
            ca_copy(step, lax.rem(me_cb - step + n_cb, n_cb)).wait_recv()
            ca_copy(step, me_cb).wait_send()
        branch = c_all[...].reshape(rows, c_all.shape[2]).astype(F32)
        for y in range(ny):
            for s in range(seqs):
                to = slice(s * length + y * part_rows, s * length + (y + 1) * part_rows)
                at = (y * seqs + s) * part_rows
                carried[to, :] = RESID * carried[to, :] + branch[at : at + part_rows]
        return 0

    lax.fori_loop(0, layers, one_layer, 0)
    out_ref[...] = carried[...].astype(out_ref.dtype)


def per_device(n_ra, n_cb, tokens, gain, gw, uw, gt, ut, gb, ub, dw):
    seqs, length, d = tokens.shape
    layers, _, ff = gw.shape
    rows = seqs * length
    nz = seqs
    ny = n_ra // nz
    pr = length // ny
    width = 256 if ff % 256 == 0 and ff // 256 >= 8 else 128
    chunks = ff // width
    dims = (n_ra, n_cb, nz, seqs, length, layers, width, chunks)
    vmem = pl.BlockSpec(memory_space=pltpu.VMEM)
    hbm = pl.BlockSpec(memory_space=pl.ANY)
    dma = pltpu.SemaphoreType.DMA
    ys, zs = max(ny - 1, 1), nz - 1
    scratch = [
        pltpu.VMEM((layers, d, ff), BF16),
        pltpu.VMEM((layers, d, ff), BF16),
        pltpu.VMEM((layers, ff, d), BF16),
        pltpu.VMEM((rows, d), F32),
        pltpu.VMEM((rows, d), BF16),
        pltpu.VMEM((rows, 128), F32),
        pltpu.VMEM((rows, width), F32),
        pltpu.VMEM((rows, d), F32),
        pltpu.VMEM((8, rows), F32),
        pltpu.VMEM((n_ra - 1, 8, rows), F32),
        pltpu.VMEM((chunks, ny, seqs, pr, 2 * width), BF16),
        pltpu.VMEM((chunks, ys, seqs, pr, 2 * width), BF16),
        pltpu.VMEM((chunks, seqs, pr, 2 * width), BF16),
        pltpu.VMEM((chunks, zs, pr, 2 * width), BF16),
        pltpu.VMEM((chunks, ny, seqs, pr, width), BF16),
        pltpu.VMEM((n_cb, rows // n_cb, d), BF16),
        pltpu.VMEM((n_cb - 1, rows // n_cb, d), BF16),
        pltpu.VMEM((n_cb, rows // n_cb, d), BF16),
        dma((layers, 3)),
        dma((n_ra - 1,)), dma((n_ra - 1,)),
        dma((chunks, ys)), dma((chunks, ys)),
        dma((chunks, zs)), dma((chunks, zs)),
        dma((chunks, zs)), dma((chunks, zs)),
        dma((chunks, ys)), dma((chunks, ys)),
        dma((n_cb - 1,)), dma((n_cb - 1,)),
        dma((n_cb - 1,)), dma((n_cb - 1,)),
    ]
    out = pl.pallas_call(
        functools.partial(kernel, dims),
        out_shape=jax.ShapeDtypeStruct((rows, d), tokens.dtype),
        in_specs=[vmem, vmem, hbm, hbm, vmem, vmem, vmem, vmem, hbm],
        out_specs=vmem,
        scratch_shapes=scratch,
        compiler_params=pltpu.CompilerParams(
            collective_id=0, has_side_effects=True, vmem_limit_bytes=60 * 1024 * 1024
        ),
        name="blocks",
    )(
        tokens.reshape(rows, d), gain[:, None, :], gw, uw, gt, ut,
        gb[:, None, :], ub[:, None, :], dw,
    )
    return out.reshape(tokens.shape)


def solution(mesh):
    in_specs = (
        P(None, None, "ra"),
        P(None, "ra"),
        P(None, "ra", "cb"),
        P(None, "ra", "cb"),
        P(None, None, "cb"),
        P(None, None, "cb"),
        P(None, "cb"),
        P(None, "cb"),
        P(None, "cb", "ra"),
    )
    return jax.shard_map(
        functools.partial(per_device, mesh.shape["ra"], mesh.shape["cb"]),
        mesh=mesh, in_specs=in_specs, out_specs=P(None, None, "ra"), check_vma=False,
    )
```

time: 540 us -> 270 us (0.50)
  waiting for transfers between devices: 425 us -> 0 us
  Pallas kernels: 0 us -> 261 us
  blocking collectives: 38.2 us -> 0 us
  other arithmetic: 34.1 us -> 0 us
  matrix products: 26 us -> 0 us
  between operations: 13.3 us -> 0.01 us
  local copies, waits for them, and re-layouts: 1.06 us -> 8.92 us
    psum x4 -> x0, waiting for transfers between devices: 425 us -> none  [the longest x2 362 us: per_device(): lax.psum(partial_value.astype(jnp.bfloat16), 'ra').astype(jnp.float32)]
    pallas_call x0 -> x1, Pallas kernels: none -> 261 us  [per_device(): pl.pallas_call(functools.partial(kernel, dims), out_shape=jax.ShapeDtypeS...]
    psum x2 -> x0, blocking collectives: 38.2 us -> none  [per_device(): row_squares = lax.psum(local_squares, 'ra')]
    dot_general x6 -> x0, matrix products: 26 us -> none  [the longest x2 13.9 us: per_device(): jnp.dot(hidden, down_local, preferred_element_type=jnp.float32)]
    add x2 -> x0, other arithmetic: 12.5 us -> none  [causal_conv(): result = result + kernel[tap_idx] * padded[:, tap_idx:tap_idx + length]]
    convert_element_type x3 -> x0, other arithmetic: 10.5 us -> none  [the longest x2 8.42 us: per_device(): projected = (summed * inverse[:, None, None]).astype(jnp.bfloat16)]
    another operation x3 -> x0, other arithmetic: 6.11 us -> none  [the longest x2 6.06 us: per_device(): jnp.stack([jnp.dot(scaled, gate_weight[layer_idx], preferred_element_type...]
  transfers between devices with their start and end apart: 4 -> 0, of which waited for: 4 -> 0; matrix products, arithmetic and copies ran while one was open for 0% -> 0% of each run, Pallas kernels for 0% -> 0%
where the time goes in v1:
time: 270 us
  Pallas kernels  261 us (97%)
  local copies, waits for them, and re-layouts  8.92 us (3%)
    pallas_call x1, Pallas kernels, per_device(): pl.pallas_call(functools.partial(kernel, dims), out_shape=jax.ShapeDtypeS...  261 us

profile of v1, /device:TPU:1, one launch (start us, length us, event | category | flops | bytes accessed | tf_op | source)
XLA Modules:
  0.0 269.8 jit_solution(3201129925167370237)
XLA Ops:
  0.0 1.3 broadcast_in_dim.9.gain_ref
  1.3 1.4 broadcast_in_dim.10.gb_ref
  2.6 1.3 broadcast_in_dim.11.ub_ref
  4.0 1.5 copy.10.gt_ref
  5.5 1.5 copy.11.ut_ref
  7.1 260.9 %blocks.1 = bf16[512,512]{1,0:T(8,128)(2,1)} custom-call(bf16[512,512]{1,0:T(8,128)(2,1)} %bitcast.3, f32[2,1,512]{2,1,0:T(1,128)} %broadcast_in_dim.9.gain_ref, bf16[2,512,2816]{2,1,0:T(8,128)(2,1)} %gw_hbm.1, bf16[2,512,2816]{2,1,0:T(8,128)(2,1)} %uw_hbm.1, f32[2,3,2816]{2,1,0:T(4,128)} %copy.10.gt_ref, f32[2,3,2816]{2,1,0:T(4,128)} %copy.11.ut_ref, ...), custom_call_target="tpu_custom_call" | custom-call | tf_op jit(solution)/shard_map/blocks/pallas_call | solution.py:278
  267.9 1.9 copy.13

commit v2 on v0

v2 whole, which is shorter than its diff:
```python
import functools

import jax
import jax.numpy as jnp
from jax import lax
from jax.experimental import pallas as pl
from jax.experimental.pallas import tpu as pltpu
from jax.sharding import PartitionSpec as P

EPS = 1e-06
RESID = 0.5
GROUPS = 2
STAGES = (("project", 0), ("add_y", 1), ("activate", 3), ("spread_y", 4), ("down", 6))
STAGES = tuple((lag, stage) for stage, lag in STAGES)
TAILS = ((0, "reduce_start"), (1, "reduce_end"), (2, "finish"), (3, "settle"))

MESH = pl.DeviceIdType.MESH
F32, BF16 = jnp.float32, jnp.bfloat16


def kernel(
    dims,
    tok_ref, gain_ref, gw_hbm, uw_hbm, gt_ref, ut_ref, gb_ref, ub_ref, dw_hbm,
    out_ref,
    gw_ref, uw_ref, dw_ref, carried, scaled, inv, tmp, acc,
    sq_own, sq_in, part, y_in, zpart, z_in, hid, c_out, c_in, c_all,
    w_sem, sq_s, sq_r, y_s, y_r, z_s, z_r, hz_s, hz_r, hy_s, hy_r, c_s, c_r, ca_s, ca_r,
):
    n_ra, n_cb, nz, groups, rows, length, layers, width, chunks = dims
    ny = n_ra // nz
    total_chunks = layers * groups * chunks
    cb_rows = rows // n_cb
    me_ra = lax.axis_index("ra")
    me_cb = lax.axis_index("cb")
    me_z, me_y = me_ra // ny, me_ra % ny

    def weight_copies(layer):
        return [
            pltpu.make_async_copy(src.at[layer], dst.at[layer], w_sem.at[layer, k])
            for k, (src, dst) in enumerate(
                [(gw_hbm, gw_ref), (uw_hbm, uw_ref), (dw_hbm, dw_ref)]
            )
        ]

    for layer in range(layers):
        for copy in weight_copies(layer):
            copy.start()

    barrier = pltpu.get_barrier_semaphore()
    for step in range(1, n_ra):
        pl.semaphore_signal(
            barrier, inc=1, device_id={"ra": lax.rem(me_ra + step, n_ra)}, device_id_type=MESH
        )
    for step in range(1, n_cb):
        pl.semaphore_signal(
            barrier, inc=1, device_id={"cb": lax.rem(me_cb + step, n_cb)}, device_id_type=MESH
        )

    def remote(src, dst, send, recv, **where):
        return pltpu.make_async_remote_copy(
            src_ref=src, dst_ref=dst, send_sem=send, recv_sem=recv,
            device_id=where, device_id_type=MESH,
        )

    def square_copy(g, step):
        return remote(
            sq_own.at[g], sq_in.at[g, step - 1], sq_s.at[g, step - 1], sq_r.at[g, step - 1],
            ra=lax.rem(me_ra + step, n_ra),
        )

    def y_copy(g, i, step):
        to = lax.rem(me_y + step, ny)
        return remote(
            part.at[g, i, to], y_in.at[g, i, step - 1],
            y_s.at[g, i, step - 1], y_r.at[g, i, step - 1], ra=me_z * ny + to,
        )

    def z_copy(g, i, step):
        to = lax.rem(me_z + step, nz)
        return remote(
            zpart.at[g, i, to], z_in.at[g, i, step - 1],
            z_s.at[g, i, step - 1], z_r.at[g, i, step - 1], ra=to * ny + me_y,
        )

    def hz_copy(g, i, step, z):
        to = lax.rem(me_z + step, nz)
        block = hid.at[g, i, me_y, z]
        return remote(
            block, block, hz_s.at[g, i, step - 1], hz_r.at[g, i, step - 1], ra=to * ny + me_y
        )

    def hy_copy(g, i, step, y):
        to = lax.rem(me_y + step, ny)
        block = hid.at[g, i, y]
        return remote(
            block, block, hy_s.at[g, i, step - 1], hy_r.at[g, i, step - 1], ra=me_z * ny + to
        )

    def c_copy(g, step):
        to = lax.rem(me_cb + step, n_cb)
        return remote(
            c_out.at[g, to], c_in.at[g, step - 1], c_s.at[g, step - 1], c_r.at[g, step - 1], cb=to
        )

    def ca_copy(g, step, block):
        to = lax.rem(me_cb + step, n_cb)
        block = c_all.at[g, block]
        return remote(block, block, ca_s.at[g, step - 1], ca_r.at[g, step - 1], cb=to)

    row_in_seq = lax.broadcasted_iota(jnp.int32, (length, width), 0)

    def prepare(layer, g):
        values = carried[g]
        squares = jnp.sum(values * values, axis=1, keepdims=True)
        sq_own[g] = jnp.transpose(jnp.broadcast_to(squares, (rows, 128)))[:8]
        for step in range(1, n_ra):
            square_copy(g, step).start()
        scaled[g] = (values * gain_ref[layer]).astype(BF16)
        acc[g] = jnp.zeros(acc.shape[1:], F32)

    def scale(g):
        total = sq_own[g]
        for step in range(1, n_ra):
            square_copy(g, step).wait()
            total = total + sq_in[g, step - 1]
        total = jnp.transpose(jnp.concatenate([total] * 16, axis=0))
        inv[g] = lax.rsqrt(total / (n_ra * gain_ref.shape[2]) + EPS)

    def project(layer, g, i):
        cols = pl.ds(pl.multiple_of(i * width, width), width)
        for half, (w_ref, taps) in enumerate([(gw_ref, gt_ref), (uw_ref, ut_ref)]):
            lanes = slice(half * width, (half + 1) * width)
            tmp[...] = jnp.dot(scaled[g], w_ref[layer, :, cols], preferred_element_type=F32)
            tap = [taps[layer, pl.ds(k, 1), cols] for k in range(3)]
            for s in range(rows // length):
                span = slice(s * length, (s + 1) * length)
                pre = tmp[span, :] * inv[g, span, :1]
                last = jnp.where(row_in_seq >= 1, pltpu.roll(pre, 1, 0), 0.0)
                older = jnp.where(row_in_seq >= 2, pltpu.roll(pre, 2, 0), 0.0)
                tmp[span, :] = tap[0] * older + tap[1] * last + tap[2] * pre
            part[g, i, :, :, :, lanes] = tmp[...].astype(BF16).reshape(
                ny, nz, rows // n_ra, width
            )
        for step in range(1, ny):
            y_copy(g, i, step).start()

    def add_y(layer, g, i):
        for step in range(1, ny):
            y_copy(g, i, step).wait_recv()
        value = part[g, i, me_y].astype(F32)
        for step in range(1, ny):
            value = value + y_in[g, i, step - 1].astype(F32)
        zpart[g, i] = value.astype(BF16)
        for step in range(1, nz):
            z_copy(g, i, step).start()

    def activate(layer, g, i):
        cols = pl.ds(pl.multiple_of(i * width, width), width)
        for step in range(1, nz):
            z_copy(g, i, step).wait_recv()
        value = zpart[g, i, me_z].astype(F32)
        for step in range(1, nz):
            value = value + z_in[g, i, step - 1].astype(F32)
        gate = value[:, :width] + gb_ref[layer, :, cols]
        up = value[:, width:] + ub_ref[layer, :, cols]
        hid[g, i, me_y, me_z] = (gate / (1.0 + jnp.exp(-gate)) * up).astype(BF16)
        for step in range(1, nz):
            hz_copy(g, i, step, me_z).start()

    def spread_y(layer, g, i):
        for step in range(1, nz):
            hz_copy(g, i, step, lax.rem(me_z - step + nz, nz)).wait_recv()
        for step in range(1, ny):
            hy_copy(g, i, step, me_y).start()

    def down(layer, g, i):
        depth = pl.ds(pl.multiple_of(i * width, width), width)
        for step in range(1, ny):
            hy_copy(g, i, step, lax.rem(me_y - step + ny, ny)).wait_recv()
        acc[g] += jnp.dot(
            hid[g, i].reshape(rows, width), dw_ref[layer, depth, :], preferred_element_type=F32
        )

    def reduce_start(layer, g):
        c_out[g] = acc[g].astype(BF16).reshape(c_out.shape[1:])
        for step in range(1, n_cb):
            c_copy(g, step).start()

    def reduce_end(layer, g):
        value = acc[g, pl.ds(pl.multiple_of(me_cb * cb_rows, cb_rows), cb_rows), :]
        for step in range(1, n_cb):
            c_copy(g, step).wait()
            value = value + c_in[g, step - 1].astype(F32)
        c_all[g, me_cb] = value.astype(BF16)
        for step in range(1, n_cb):
            ca_copy(g, step, me_cb).start()

    def finish(layer, g):
        for step in range(1, n_cb):
            ca_copy(g, step, lax.rem(me_cb - step + n_cb, n_cb)).wait_recv()
            ca_copy(g, step, me_cb).wait_send()
        branch = c_all[g].reshape(rows, c_all.shape[3]).astype(F32)
        carried[g] = RESID * carried[g] + branch

        @pl.when(layer < layers - 1)
        def _():
            prepare(layer + 1, g)

    def settle(layer, g):
        def one(i, _):
            for step in range(1, ny):
                y_copy(g, i, step).wait_send()
                hy_copy(g, i, step, me_y).wait_send()
            for step in range(1, nz):
                z_copy(g, i, step).wait_send()
                hz_copy(g, i, step, me_z).wait_send()
            return 0

        lax.fori_loop(0, chunks, one, 0)

        @pl.when(layer < layers - 1)
        def _():
            scale(g)

    carried[...] = tok_ref[...].astype(F32)
    pl.semaphore_wait(barrier, n_ra + n_cb - 2)
    for g in range(groups):
        prepare(0, g)
    for layer in range(layers):
        for copy in weight_copies(layer):
            copy.wait()
    for g in range(groups):
        scale(g)

    def body(t, _):
        for lag, stage in STAGES:
            at = t - lag
            run = at // chunks

            @pl.when((at >= 0) & (at < total_chunks))
            def _():
                stage_of[stage](run // groups, run % groups, at % chunks)

        for lag, stage in TAILS:
            at = t - STAGES[-1][0] - lag
            run = at // chunks

            @pl.when((at >= 0) & (at < total_chunks) & (at % chunks == chunks - 1))
            def _():
                stage_of[stage](run // groups, run % groups)

        return 0

    stage_of = {
        "project": project, "add_y": add_y, "activate": activate, "spread_y": spread_y,
        "down": down, "reduce_start": reduce_start, "reduce_end": reduce_end,
        "finish": finish, "settle": settle,
    }
    lax.fori_loop(0, total_chunks + STAGES[-1][0] + TAILS[-1][0], body, 0)
    out_ref[...] = carried[...].astype(out_ref.dtype)


def per_device(n_ra, n_cb, tokens, gain, gw, uw, gt, ut, gb, ub, dw):
    seqs, length, d = tokens.shape
    layers, _, ff = gw.shape
    nz = seqs
    ny = n_ra // nz
    groups = GROUPS
    rows = seqs * length // groups
    pr = rows // n_ra
    width = 256 if ff % 256 == 0 and ff // 256 >= 8 else 128
    chunks = ff // width
    dims = (n_ra, n_cb, nz, groups, rows, length, layers, width, chunks)
    vmem = pl.BlockSpec(memory_space=pltpu.VMEM)
    hbm = pl.BlockSpec(memory_space=pl.ANY)
    dma = pltpu.SemaphoreType.DMA
    ys, zs = max(ny - 1, 1), nz - 1
    scratch = [
        pltpu.VMEM((layers, d, ff), BF16),
        pltpu.VMEM((layers, d, ff), BF16),
        pltpu.VMEM((layers, ff, d), BF16),
        pltpu.VMEM((groups, rows, d), F32),
        pltpu.VMEM((groups, rows, d), BF16),
        pltpu.VMEM((groups, rows, 128), F32),
        pltpu.VMEM((rows, width), F32),
        pltpu.VMEM((groups, rows, d), F32),
        pltpu.VMEM((groups, 8, rows), F32),
        pltpu.VMEM((groups, n_ra - 1, 8, rows), F32),
        pltpu.VMEM((groups, chunks, ny, nz, pr, 2 * width), BF16),
        pltpu.VMEM((groups, chunks, ys, nz, pr, 2 * width), BF16),
        pltpu.VMEM((groups, chunks, nz, pr, 2 * width), BF16),
        pltpu.VMEM((groups, chunks, zs, pr, 2 * width), BF16),
        pltpu.VMEM((groups, chunks, ny, nz, pr, width), BF16),
        pltpu.VMEM((groups, n_cb, rows // n_cb, d), BF16),
        pltpu.VMEM((groups, n_cb - 1, rows // n_cb, d), BF16),
        pltpu.VMEM((groups, n_cb, rows // n_cb, d), BF16),
        dma((layers, 3)),
        dma((groups, n_ra - 1)), dma((groups, n_ra - 1)),
        dma((groups, chunks, ys)), dma((groups, chunks, ys)),
        dma((groups, chunks, zs)), dma((groups, chunks, zs)),
        dma((groups, chunks, zs)), dma((groups, chunks, zs)),
        dma((groups, chunks, ys)), dma((groups, chunks, ys)),
        dma((groups, n_cb - 1)), dma((groups, n_cb - 1)),
        dma((groups, n_cb - 1)), dma((groups, n_cb - 1)),
    ]
    out = pl.pallas_call(
        functools.partial(kernel, dims),
        out_shape=jax.ShapeDtypeStruct((groups, rows, d), tokens.dtype),
        in_specs=[vmem, vmem, hbm, hbm, vmem, vmem, vmem, vmem, hbm],
        out_specs=vmem,
        scratch_shapes=scratch,
        compiler_params=pltpu.CompilerParams(
            collective_id=0, has_side_effects=True, vmem_limit_bytes=60 * 1024 * 1024
        ),
        name="blocks",
    )(
        tokens.reshape(groups, rows, d), gain[:, None, :], gw, uw, gt, ut,
        gb[:, None, :], ub[:, None, :], dw,
    )
    return out.reshape(tokens.shape)


def solution(mesh):
    in_specs = (
        P(None, None, "ra"),
        P(None, "ra"),
        P(None, "ra", "cb"),
        P(None, "ra", "cb"),
        P(None, None, "cb"),
        P(None, None, "cb"),
        P(None, "cb"),
        P(None, "cb"),
        P(None, "cb", "ra"),
    )
    return jax.shard_map(
        functools.partial(per_device, mesh.shape["ra"], mesh.shape["cb"]),
        mesh=mesh, in_specs=in_specs, out_specs=P(None, None, "ra"), check_vma=False,
    )
```

time: 540 us -> 242 us (0.45)
  waiting for transfers between devices: 425 us -> 0 us
  Pallas kernels: 0 us -> 232 us
  blocking collectives: 38.2 us -> 0 us
  other arithmetic: 34.1 us -> 0 us
  matrix products: 26 us -> 0 us
  between operations: 13.3 us -> 0.01 us
  local copies, waits for them, and re-layouts: 1.06 us -> 8.92 us
    psum x4 -> x0, waiting for transfers between devices: 425 us -> none  [the longest x2 362 us: per_device(): lax.psum(partial_value.astype(jnp.bfloat16), 'ra').astype(jnp.float32)]
    pallas_call x0 -> x1, Pallas kernels: none -> 232 us  [per_device(): pl.pallas_call(functools.partial(kernel, dims), out_shape=jax.ShapeDtypeS...]
    psum x2 -> x0, blocking collectives: 38.2 us -> none  [per_device(): row_squares = lax.psum(local_squares, 'ra')]
    dot_general x6 -> x0, matrix products: 26 us -> none  [the longest x2 13.9 us: per_device(): jnp.dot(hidden, down_local, preferred_element_type=jnp.float32)]
    add x2 -> x0, other arithmetic: 12.5 us -> none  [causal_conv(): result = result + kernel[tap_idx] * padded[:, tap_idx:tap_idx + length]]
    convert_element_type x3 -> x0, other arithmetic: 10.5 us -> none  [the longest x2 8.42 us: per_device(): projected = (summed * inverse[:, None, None]).astype(jnp.bfloat16)]
    another operation x3 -> x0, other arithmetic: 6.11 us -> none  [the longest x2 6.06 us: per_device(): jnp.stack([jnp.dot(scaled, gate_weight[layer_idx], preferred_element_type...]
  transfers between devices with their start and end apart: 4 -> 0, of which waited for: 4 -> 0; matrix products, arithmetic and copies ran while one was open for 0% -> 0% of each run, Pallas kernels for 0% -> 0%
where the time goes in v2:
time: 242 us; the launch traced here: 241 us
  Pallas kernels  232 us (96%)
  local copies, waits for them, and re-layouts  8.92 us (4%)
    pallas_call x1, Pallas kernels, per_device(): pl.pallas_call(functools.partial(kernel, dims), out_shape=jax.ShapeDtypeS...  232 us
    unnamed x3, local copies, waits for them, and re-layouts  4.95 us

profile of v2, /device:TPU:1, one launch (start us, length us, event | category | flops | bytes accessed | tf_op | source)
XLA Modules:
  0.0 241.2 jit_solution(2987269975880188775)
XLA Ops:
  0.0 1.3 broadcast_in_dim.9.gain_ref
  1.3 1.4 broadcast_in_dim.10.gb_ref
  2.6 1.3 broadcast_in_dim.11.ub_ref
  4.0 1.5 copy.10.gt_ref
  5.5 1.5 copy.11.ut_ref
  7.1 232.3 %blocks.1 = bf16[2,256,512]{2,1,0:T(8,128)(2,1)} custom-call(bf16[2,256,512]{2,1,0:T(8,128)(2,1)} %bitcast.3, f32[2,1,512]{2,1,0:T(1,128)} %broadcast_in_dim.9.gain_ref, bf16[2,512,2816]{2,1,0:T(8,128)(2,1)} %gw_hbm.1, bf16[2,512,2816]{2,1,0:T(8,128)(2,1)} %uw_hbm.1, f32[2,3,2816]{2,1,0:T(4,128)} %copy.10.gt_ref, f32[2,3,2816]{2,1,0:T(4,128)} %copy.11.ut_ref, ...), custom_call_target="tpu_custom_call" | custom-call | tf_op jit(solution)/shard_map/blocks/pallas_call | solution.py:306
  239.3 1.9 copy.13

commit v3 on v2

--- a/solution.py
+++ b/solution.py
@@ -10,7 +10,8 @@
 EPS = 1e-06
 RESID = 0.5
 GROUPS = 2
-STAGES = (("project", 0), ("add_y", 1), ("activate", 3), ("spread_y", 4), ("down", 6))
+STAGES = (("project", 0), ("add_y", 2), ("fold", 3), ("activate", 4),
+          ("spread_z", 5), ("spread_y", 6), ("down", 8))
 STAGES = tuple((lag, stage) for stage, lag in STAGES)
 TAILS = ((0, "reduce_start"), (1, "reduce_end"), (2, "finish"), (3, "settle"))
 
@@ -23,7 +24,7 @@
     tok_ref, gain_ref, gw_hbm, uw_hbm, gt_ref, ut_ref, gb_ref, ub_ref, dw_hbm,
     out_ref,
     gw_ref, uw_ref, dw_ref, carried, scaled, inv, tmp, acc,
-    sq_own, sq_in, part, y_in, zpart, z_in, hid, c_out, c_in, c_all,
+    sq_own, sq_in, part, y_in, zpart, z_in, zfold, zf_in, hid, c_out, c_in, c_all,
     w_sem, sq_s, sq_r, y_s, y_r, z_s, z_r, hz_s, hz_r, hy_s, hy_r, c_s, c_r, ca_s, ca_r,
 ):
     n_ra, n_cb, nz, groups, rows, length, layers, width, chunks = dims
@@ -75,19 +76,30 @@
             y_s.at[g, i, step - 1], y_r.at[g, i, step - 1], ra=me_z * ny + to,
         )
 
-    def z_copy(g, i, step):
-        to = lax.rem(me_z + step, nz)
-        return remote(
-            zpart.at[g, i, to], z_in.at[g, i, step - 1],
-            z_s.at[g, i, step - 1], z_r.at[g, i, step - 1], ra=to * ny + me_y,
-        )
-
-    def hz_copy(g, i, step, z):
-        to = lax.rem(me_z + step, nz)
-        block = hid.at[g, i, me_y, z]
-        return remote(
-            block, block, hz_s.at[g, i, step - 1], hz_r.at[g, i, step - 1], ra=to * ny + me_y
-        )
+    side, half_z = me_z % 2, me_z // 2
+    my_block = 2 * side + half_z
+    near = (me_z + 1 - 2 * side) * ny + me_y
+    far = (me_z + 2 - 4 * half_z) * ny + me_y
+
+    def near_copy(g, i):
+        return remote(
+            zpart.at[g, i, pl.ds(2 * (1 - side), 2)], z_in.at[g, i],
+            z_s.at[g, i, 0], z_r.at[g, i, 0], ra=near,
+        )
+
+    def far_copy(g, i):
+        return remote(
+            zfold.at[g, i, 1 - half_z], zf_in.at[g, i],
+            z_s.at[g, i, 1], z_r.at[g, i, 1], ra=far,
+        )
+
+    def hfar_copy(g, i, block):
+        block = hid.at[g, i, me_y, block]
+        return remote(block, block, hz_s.at[g, i, 0], hz_r.at[g, i, 0], ra=far)
+
+    def hnear_copy(g, i, first):
+        block = hid.at[g, i, me_y, pl.ds(2 * first, 2)]
+        return remote(block, block, hz_s.at[g, i, 1], hz_r.at[g, i, 1], ra=near)
 
     def hy_copy(g, i, step, y):
         to = lax.rem(me_y + step, ny)
@@ -151,25 +163,29 @@
         for step in range(1, ny):
             value = value + y_in[g, i, step - 1].astype(F32)
         zpart[g, i] = value.astype(BF16)
-        for step in range(1, nz):
-            z_copy(g, i, step).start()
+        near_copy(g, i).start()
+
+    def fold(layer, g, i):
+        near_copy(g, i).wait_recv()
+        value = zpart[g, i, pl.ds(2 * side, 2)].astype(F32) + z_in[g, i].astype(F32)
+        zfold[g, i] = value.astype(BF16)
+        far_copy(g, i).start()
 
     def activate(layer, g, i):
         cols = pl.ds(pl.multiple_of(i * width, width), width)
-        for step in range(1, nz):
-            z_copy(g, i, step).wait_recv()
-        value = zpart[g, i, me_z].astype(F32)
-        for step in range(1, nz):
-            value = value + z_in[g, i, step - 1].astype(F32)
+        far_copy(g, i).wait_recv()
+        value = zfold[g, i, half_z].astype(F32) + zf_in[g, i].astype(F32)
         gate = value[:, :width] + gb_ref[layer, :, cols]
         up = value[:, width:] + ub_ref[layer, :, cols]
-        hid[g, i, me_y, me_z] = (gate / (1.0 + jnp.exp(-gate)) * up).astype(BF16)
-        for step in range(1, nz):
-            hz_copy(g, i, step, me_z).start()
+        hid[g, i, me_y, my_block] = (gate / (1.0 + jnp.exp(-gate)) * up).astype(BF16)
+        hfar_copy(g, i, my_block).start()
+
+    def spread_z(layer, g, i):
+        hfar_copy(g, i, 2 * side + 1 - half_z).wait_recv()
+        hnear_copy(g, i, side).start()
 
     def spread_y(layer, g, i):
-        for step in range(1, nz):
-            hz_copy(g, i, step, lax.rem(me_z - step + nz, nz)).wait_recv()
+        hnear_copy(g, i, 1 - side).wait_recv()
         for step in range(1, ny):
             hy_copy(g, i, step, me_y).start()
 
@@ -211,9 +227,10 @@
             for step in range(1, ny):
                 y_copy(g, i, step).wait_send()
                 hy_copy(g, i, step, me_y).wait_send()
-            for step in range(1, nz):
-                z_copy(g, i, step).wait_send()
-                hz_copy(g, i, step, me_z).wait_send()
+            near_copy(g, i).wait_send()
+            far_copy(g, i).wait_send()
+            hfar_copy(g, i, my_block).wait_send()
+            hnear_copy(g, i, side).wait_send()
             return 0
 
         lax.fori_loop(0, chunks, one, 0)
@@ -252,7 +269,8 @@
         return 0
 
     stage_of = {
-        "project": project, "add_y": add_y, "activate": activate, "spread_y": spread_y,
+        "project": project, "add_y": add_y, "activate": activate, "spread_z": spread_z,
+        "spread_y": spread_y, "fold": fold,
         "down": down, "reduce_start": reduce_start, "reduce_end": reduce_end,
         "finish": finish, "settle": settle,
     }
@@ -274,7 +292,7 @@
     vmem = pl.BlockSpec(memory_space=pltpu.VMEM)
     hbm = pl.BlockSpec(memory_space=pl.ANY)
     dma = pltpu.SemaphoreType.DMA
-    ys, zs = max(ny - 1, 1), nz - 1
+    ys, zs = max(ny - 1, 1), 2
     scratch = [
         pltpu.VMEM((layers, d, ff), BF16),
         pltpu.VMEM((layers, d, ff), BF16),
@@ -289,7 +307,9 @@
         pltpu.VMEM((groups, chunks, ny, nz, pr, 2 * width), BF16),
         pltpu.VMEM((groups, chunks, ys, nz, pr, 2 * width), BF16),
         pltpu.VMEM((groups, chunks, nz, pr, 2 * width), BF16),
-        pltpu.VMEM((groups, chunks, zs, pr, 2 * width), BF16),
+        pltpu.VMEM((groups, chunks, 2, pr, 2 * width), BF16),
+        pltpu.VMEM((groups, chunks, 2, pr, 2 * width), BF16),
+        pltpu.VMEM((groups, chunks, pr, 2 * width), BF16),
         pltpu.VMEM((groups, chunks, ny, nz, pr, width), BF16),
         pltpu.VMEM((groups, n_cb, rows // n_cb, d), BF16),
         pltpu.VMEM((groups, n_cb - 1, rows // n_cb, d), BF16),

time: 242 us -> 231 us (0.955)
  Pallas kernels: 232 us -> 221 us
    pallas_call x1, Pallas kernels: 232 us -> 221 us  [per_device(): pl.pallas_call(functools.partial(kernel, dims), out_shape=jax.ShapeDtypeS...]
where the time goes in v3:
time: 231 us; the launch traced here: 230 us
  Pallas kernels  221 us (96%)
  local copies, waits for them, and re-layouts  8.92 us (4%)
    pallas_call x1, Pallas kernels, per_device(): pl.pallas_call(functools.partial(kernel, dims), out_shape=jax.ShapeDtypeS...  221 us
    unnamed x3, local copies, waits for them, and re-layouts  4.95 us

profile of v3, /device:TPU:1, one launch (start us, length us, event | category | flops | bytes accessed | tf_op | source)
XLA Modules:
  0.0 230.2 jit_solution(826911339458033719)
XLA Ops:
  0.0 1.3 broadcast_in_dim.9.gain_ref
  1.3 1.4 broadcast_in_dim.10.gb_ref
  2.6 1.3 broadcast_in_dim.11.ub_ref
  4.0 1.5 copy.10.gt_ref
  5.5 1.5 copy.11.ut_ref
  7.1 221.3 %blocks.1 = bf16[2,256,512]{2,1,0:T(8,128)(2,1)} custom-call(bf16[2,256,512]{2,1,0:T(8,128)(2,1)} %bitcast.3, f32[2,1,512]{2,1,0:T(1,128)} %broadcast_in_dim.9.gain_ref, bf16[2,512,2816]{2,1,0:T(8,128)(2,1)} %gw_hbm.1, bf16[2,512,2816]{2,1,0:T(8,128)(2,1)} %uw_hbm.1, f32[2,3,2816]{2,1,0:T(4,128)} %copy.10.gt_ref, f32[2,3,2816]{2,1,0:T(4,128)} %copy.11.ut_ref, ...), custom_call_target="tpu_custom_call" | custom-call | tf_op jit(solution)/shard_map/blocks/pallas_call | solution.py:326
  228.4 1.9 copy.13
